TPU v7x, 512 devices: a whole 4x8x8 slice. The times are simulated.
512 devices in a mesh: ep: 32 (over z, x), tp: 16 (over y, core).
Axes of the slice: x: 4, y: 8, z: 8, core: 2. Of those that a mesh axis runs over, the one named last changes fastest.
Arguments:
- tokens: bfloat16 [256, 4096], P('ep', 'tp'), may hold values from -6 to 6
- norm_gain: float32 [4096], replicated, may hold values from 0.1 to 1.9
- route_experts: int32 [256, 2], P('ep'), may hold values from 0 to 63, all different within a row; in each aligned block of 8 rows (0 to 7, 8 to 15, ...) at most 2 rows name the same one
- route_logits: float32 [256, 2], P('ep'), may hold values from -4 to 4
- expert_gate: bfloat16 [64, 4096, 1024], P('ep', None, 'tp'), may hold values from -0.09375 to 0.09375
- expert_up: bfloat16 [64, 4096, 1024], P('ep', None, 'tp'), may hold values from -0.09375 to 0.09375
- expert_down: bfloat16 [64, 1024, 4096], P('ep', 'tp'), may hold values from -0.1875 to 0.1875
- dense_gate: bfloat16 [4096, 1024], P(None, 'tp'), may hold values from -0.09375 to 0.09375
- dense_up: bfloat16 [4096, 1024], P(None, 'tp'), may hold values from -0.09375 to 0.09375
- dense_down: bfloat16 [1024, 4096], P('tp'), may hold values from -0.1875 to 0.1875
- mix_weight: float32 [4096], replicated, may hold values from -0.09375 to 0.09375
- out_gain: float32 [4096], P('tp'), may hold values from 0.1 to 1.9
Outputs:
- result: bfloat16 [256, 4096], P('ep', 'tp')
Inputs may be any that keep to these rules, and one draw needn't show every extreme that they name: `route_experts`: each row names 2 different experts; the 8 rows of one index of ep (aligned blocks) name any one expert at most 2 times, and some block names some expert exactly 2 times; every expert is named somewhere.
All inputs are finite; a program needn't handle non-finite values.
Results may differ from a plain program's by a relative error of at most 0.0025.
Values may be sent and summed in bfloat16 or wider, within the bound.
A program may use at most 64 MiB of HBM per device.

v0:
```python
import jax
import jax.numpy as jnp
from jax import lax
from jax.sharding import Mesh
from jax.sharding import PartitionSpec as P

CAP = 2
TP = ("tp_0", "tp_1")
norm_eps = 1e-06


def summed_rows(x, axes, dim):
    if not axes:
        return x
    nearer = lax.psum_scatter(x, axes[0], scatter_dimension=dim, tiled=True)
    return summed_rows(nearer, axes[1:], dim)


def local(
    tokens,
    norm_gain,
    route_experts,
    route_logits,
    expert_gate,
    expert_up,
    expert_down,
    dense_gate,
    dense_up,
    dense_down,
    mix_weight,
    out_gain,
):
    tok_rows, width_part = tokens.shape
    groups = lax.axis_size(TP)
    width = width_part * groups
    whole_rows = lax.all_gather(tokens, TP, axis=1, tiled=True).astype(jnp.float32)
    normed = (
        whole_rows
        * lax.rsqrt(jnp.mean(whole_rows * whole_rows, axis=1, keepdims=True) + norm_eps)
        * norm_gain
    ).astype(jnp.bfloat16)
    weights = jax.nn.softmax(route_logits, axis=-1)
    top_count = route_experts.shape[1]
    local_experts = expert_gate.shape[0]
    peer_count = lax.axis_size("ep")
    experts = local_experts * peer_count
    dense_hidden = (
        jax.nn.silu(jnp.dot(normed, dense_gate, preferred_element_type=jnp.float32))
        * jnp.dot(normed, dense_up, preferred_element_type=jnp.float32)
    ).astype(jnp.bfloat16)
    dense_out = summed_rows(
        jnp.dot(dense_hidden, dense_down, preferred_element_type=jnp.float32), TP, 1
    )
    mix_gate = jax.nn.sigmoid(
        jnp.dot(normed.astype(jnp.float32), mix_weight, precision=lax.Precision.HIGHEST)
    )
    flat_routes = route_experts.reshape(-1)
    expert_ids = jnp.arange(experts, dtype=jnp.int32)
    capacity = CAP
    slot_count = experts * capacity
    route_hits = (flat_routes[:, None] == expert_ids[None, :]).astype(jnp.int32)
    before = jnp.cumsum(route_hits, axis=0) - route_hits
    slot_rank = jnp.sum(before * route_hits, axis=1)
    position = flat_routes * capacity + slot_rank
    onehot_place = (position[:, None] == jnp.arange(slot_count, dtype=jnp.int32)[None, :]).astype(
        jnp.float32
    )
    placing = jnp.sum(onehot_place.reshape(tok_rows, top_count, slot_count), axis=1).T.astype(
        jnp.bfloat16
    )
    outgoing = jnp.dot(placing, normed, preferred_element_type=jnp.float32).astype(jnp.bfloat16)
    received = lax.all_to_all(outgoing, "ep", split_axis=0, concat_axis=0, tiled=True)
    arranged = (
        received.reshape(peer_count, local_experts, capacity, width)
        .transpose(1, 0, 2, 3)
        .reshape(local_experts, peer_count * capacity, width)
    )
    gate_act = jnp.einsum("erd,edf->erf", arranged, expert_gate, preferred_element_type=jnp.float32)
    up_act = jnp.einsum("erd,edf->erf", arranged, expert_up, preferred_element_type=jnp.float32)
    hidden = (jax.nn.silu(gate_act) * up_act).astype(jnp.bfloat16)
    partial_value = jnp.einsum(
        "erf,efd->erd", hidden, expert_down, preferred_element_type=jnp.float32
    )
    summed = lax.psum_scatter(partial_value, TP, scatter_dimension=2, tiled=True)
    back_send = (
        summed.reshape(local_experts, peer_count, capacity, width_part)
        .transpose(1, 0, 2, 3)
        .reshape(slot_count, width_part)
    )
    returned = lax.all_to_all(back_send, "ep", split_axis=0, concat_axis=0, tiled=True)
    combine_map = jnp.sum(
        (onehot_place * weights.reshape(-1)[:, None]).reshape(tok_rows, top_count, slot_count),
        axis=1,
    )
    expert_mix = jnp.dot(combine_map, returned, precision=lax.Precision.HIGHEST)
    combined = expert_mix + mix_gate[:, None] * dense_out
    squares_out = lax.psum(jnp.sum(combined * combined, axis=1), TP)
    result = combined * lax.rsqrt(squares_out[:, None] / width + norm_eps) * out_gain
    return result.astype(jnp.bfloat16)


def solution(mesh):
    split = Mesh(mesh.devices.reshape(mesh.shape["ep"], 8, 2), ("ep", "tp_0", "tp_1"))
    in_specs = (
        P("ep", TP),
        P(),
        P("ep", None),
        P("ep", None),
        P("ep", None, TP),
        P("ep", None, TP),
        P("ep", TP, None),
        P(None, TP),
        P(None, TP),
        P(TP, None),
        P(),
        P(TP),
    )
    out_specs = P("ep", TP)
    return jax.shard_map(local, mesh=split, in_specs=in_specs, out_specs=out_specs, check_vma=False)
```

profile of v0, /device:TPU:2, one launch (start us, length us, event | category | flops | bytes accessed | tf_op | source)
XLA Modules:
  0.0 229.2 jit_solution(5264460515615627035)
XLA Ops:
  6.5 0.8 reduce_max.9
  7.3 0.7 fusion.26
  8.0 0.7 fusion.25
  8.7 0.8 copy.34
  9.5 0.1 eq.30
  9.6 0.1 fusion.17
  9.7 0.2 select_reduce_fusion.1
  9.8 0.1 reduce_sum.57
  9.9 0.1 copy.36
  10.0 18.0 %all_gather.3 = bf16[8,4096]{1,0:T(8,128)(2,1)S(1)} all-gather(bf16[8,256]{1,0:T(8,128)(2,1)} %param.12), channel_id=1, replica_groups=mesh['ep'=32,'tp_0'=8,'tp_1'=2] {'tp_0','tp_1'}, dimensions={1}, use_global_device_ids=true | all-gather | bytes 69632 | tf_op jit(solution)/shard_map/all_gather | solution.py:36
  28.0 0.1 fusion.8
  28.2 1.2 convolution_convert_fusion
  29.5 0.4 all_to_all.14
  29.9 41.8 %all_to_all.21 = bf16[32,4,4096]{2,1,0:T(4,128)(2,1)S(1)} all-to-all(bf16[32,4,4096]{2,1,0:T(4,128)(2,1)S(1)} %all_to_all.14), channel_id=1, replica_groups=mesh['ep'=32,'tp_0'=8,'tp_1'=2] {'ep'}, dimensions={0} | all-to-all | bytes 2097152 | tf_op jit(solution)/shard_map/all_to_all | solution.py:72
  71.7 0.5 reshape.67
  72.3 2.0 copy.41
  74.3 1.6 reshape.68
  75.9 0.4 fusion.35
  76.3 3.4 %fusion.1 = f32[2,64,4096]{2,1,0:T(8,128)} fusion(bf16[2,64,4096]{2,1,0:T(8,128)(2,1)S(1)} %copy-done, bf16[2,64,4096]{2,1,0:T(8,128)(2,1)S(1)} %reshape.68, bf16[2,4096,64]{1,2,0:T(8,128)(2,1)} %param.17, f32[2,64,64]{2,1,0:T(8,128)S(1)} %fusion.35), kind=kOutput, calls=%fused_computation.3 | convolution fusion | flops 134266880 | bytes 5275648 | tf_op jit(solution)/shard_map/erf,efd->erd/dot_general | solution.py:81
  79.8 0.9 copy-done.2
  80.7 0.3 fusion.31
  81.1 1.3 fusion.3
  82.4 53.8 %reduce-scatter.4.cloned.1.call-done = f32[2,64,256]{2,1,0:T(8,128)} async-done(((f32[2,64,4096]{2,1,0:T(8,128)}), f32[2,64,256]{2,1,0:T(8,128)}) %reduce-scatter.4.cloned.1.call-update) | async-done | bytes 131088 | tf_op jit(solution)/shard_map/reduce_scatter | solution.py:84
  136.1 1.0 reshape.69
  137.1 0.7 copy.39
  137.8 10.5 %all-to-all-start.1 = ((f32[32,4,256]{2,1,0:T(4,128)}), f32[32,4,256]{2,1,0:T(4,128)S(1)}, u32[]{:S(2)}, u32[]{:S(2)}) async-start(f32[32,4,256]{2,1,0:T(4,128)} %copy.39), calls=%async_computation.2 | async-start | bytes 262144 | tf_op jit(solution)/shard_map/all_to_all | solution.py:90
  148.4 28.9 %reduce-scatter.6.cloned.1.call-done = f32[8,512]{1,0:T(8,128)} async-done(((f32[8,4096]{1,0:T(8,128)}), f32[8,512]{1,0:T(8,128)}) %reduce-scatter.6.cloned.1.call-update) | async-done | bytes 16400 | tf_op jit(solution)/shard_map/reduce_scatter | solution.py:15
  177.3 0.3 fusion.7
  177.7 16.9 %reduce-scatter.8.cloned.1.call-done = f32[8,256]{1,0:T(8,128)} async-done(((f32[8,512]{1,0:T(8,128)}), f32[8,256]{1,0:T(8,128)}) %reduce-scatter.8.cloned.1.call-update) | async-done | bytes 8208 | tf_op jit(solution)/shard_map/reduce_scatter | solution.py:15
  194.6 1.0 multiply_reduce_fusion
  195.6 26.3 %psum.7 = f32[8]{0:T(128)S(1)} all-reduce(f32[8]{0:T(128)S(1)} %get-tuple-element.7), channel_id=1, replica_groups=mesh['ep'=32,'tp_0'=8,'tp_1'=2] {'tp_0','tp_1'}, use_global_device_ids=true, to_apply=%region_11.12 | all-reduce | flops 8 | bytes 64 | tf_op jit(solution)/shard_map/psum | solution.py:97
  222.0 0.7 multiply_convert_fusion
  (29 shorter events, 0.4 us)
Async XLA Ops:
  6.5 69.8 %copy-start = (bf16[2,64,4096]{2,1,0:T(8,128)(2,1)S(1)}, bf16[2,64,4096]{2,1,0:T(8,128)(2,1)}, u32[]{:S(2)}) copy-start(bf16[2,64,4096]{2,1,0:T(8,128)(2,1)} %param.18) | copy-start | bytes 3145732
  6.5 129.6 %reduce-scatter.4.cloned.1.call-start = ((), (), s32[]{:S(2)}) async-start(), calls=%async_computation.5 | async-start | bytes 2228224 | tf_op jit(solution)/shard_map/reduce_scatter | solution.py:84
  74.3 1.6 copy-start.1
  79.7 1.0 copy-start.2
  79.7 1.0 copy-start.5
  79.7 1.3 copy-start.3
  79.7 1.4 copy-start.4
  79.7 97.6 %copy-start.7 = (f32[4096]{0:T(1024)S(1)}, f32[4096]{0:T(1024)}, u32[]{:S(2)}) copy-start(f32[4096]{0:T(1024)} %param.22) | copy-start | bytes 49156
  79.7 142.2 %copy-start.6 = (f32[256]{0:T(256)S(1)}, f32[256]{0:T(256)}, u32[]{:S(2)}) copy-start(f32[256]{0:T(256)} %param.23) | copy-start | bytes 3076
  79.8 97.6 %reduce-scatter.6.cloned.1.call-start = ((), (), s32[]{:S(2)}) async-start(), calls=%async_computation.6 | async-start | bytes 147456 | tf_op jit(solution)/shard_map/reduce_scatter | solution.py:15
  137.8 39.8 %all-to-all-start.1 = ((f32[32,4,256]{2,1,0:T(4,128)}), f32[32,4,256]{2,1,0:T(4,128)S(1)}, u32[]{:S(2)}, u32[]{:S(2)}) async-start(f32[32,4,256]{2,1,0:T(4,128)} %copy.39), calls=%async_computation.2 | async-start | bytes 262144 | tf_op jit(solution)/shard_map/all_to_all | solution.py:90
  148.3 46.3 %reduce-scatter.8.cloned.1.call-start = ((), (), s32[]{:S(2)}) async-start(), calls=%async_computation.7 | async-start | bytes 24576 | tf_op jit(solution)/shard_map/reduce_scatter | solution.py:15
Sparse Core Ops, SparseCore 0:
  79.9 56.2 reduce-scatter.3
  138.9 38.3 reduce-scatter.5
  180.0 14.5 reduce-scatter.7
where the time goes:
time: 230 us; the launch traced here: 229 us
  waiting for transfers between devices  99.7 us (43%)
  blocking collectives  86.2 us (37%)
  between operations  13.2 us (6%)
  starting transfers between devices  10.6 us (5%)
  local copies, waits for them, and re-layouts  8.3 us (4%)
  matrix products  7.8 us (3%)
  other arithmetic  3.38 us (1%)
    reduce_scatter x1, waiting for transfers between devices, local(): lax.psum_scatter(partial_value, TP, scatter_dimension=2, tiled=True)  53.8 us
    reduce_scatter x2, waiting for transfers between devices, summed_rows(): nearer = lax.psum_scatter(x, axes[0], scatter_dimension=dim, tiled=True)  45.8 us
    all_to_all x1, blocking collectives, local(): lax.all_to_all(outgoing, 'ep', split_axis=0, concat_axis=0, tiled=True)  41.8 us
    psum x1, blocking collectives, local(): squares_out = lax.psum(jnp.sum(combined * combined, axis=1), TP)  26.3 us
    all_gather x1, blocking collectives, local(): lax.all_gather(tokens, TP, axis=1, tiled=True).astype(jnp.float32)  18 us
    all_to_all x1, starting transfers between devices, local(): lax.all_to_all(back_send, 'ep', split_axis=0, concat_axis=0, tiled=True)  10.5 us
  transfers between devices with their start and end apart: 4, of which 3 were waited for; matrix products, arithmetic and copies ran while one was open for 2% of the time, Pallas kernels for 0%

commit v1 on v0

--- a/solution.py
+++ b/solution.py
@@ -33,7 +33,9 @@
     tok_rows, width_part = tokens.shape
     groups = lax.axis_size(TP)
     width = width_part * groups
-    whole_rows = lax.all_gather(tokens, TP, axis=1, tiled=True).astype(jnp.float32)
+    whole_rows = jnp.concatenate(
+        lax.all_to_all(jnp.stack([tokens] * lax.axis_size(TP)), TP, 0, 0), axis=1
+    ).astype(jnp.float32)
     normed = (
         whole_rows
         * lax.rsqrt(jnp.mean(whole_rows * whole_rows, axis=1, keepdims=True) + norm_eps)

time: 230 us -> 223 us (0.970)
  blocking collectives: 86.2 us -> 68.2 us
  starting transfers between devices: 10.6 us -> 18 us
    all_gather x1 -> x0, blocking collectives: 18 us -> none  [local(): lax.all_gather(tokens, TP, axis=1, tiled=True).astype(jnp.float32)]
    all_to_all x0 -> x1, starting transfers between devices: none -> 7.21 us  [local(): lax.all_to_all(jnp.stack([tokens] * lax.axis_size(TP)), TP, 0, 0)]
    all_to_all x0 -> x1, waiting for transfers between devices: none -> 4.26 us  [local(): lax.all_to_all(jnp.stack([tokens] * lax.axis_size(TP)), TP, 0, 0)]
  transfers between devices with their start and end apart: 4 -> 5, of which waited for: 3 -> 4; matrix products, arithmetic and copies ran while one was open for 2% -> 3% of each run, Pallas kernels for 0% -> 0%
where the time goes in v1:
time: 223 us
  waiting for transfers between devices  102 us (46%)
  blocking collectives  68.2 us (31%)
  starting transfers between devices  18 us (8%)
  between operations  13.3 us (6%)
  local copies, waits for them, and re-layouts  9.73 us (4%)
  matrix products  6.91 us (3%)
  other arithmetic  4.12 us (2%)
    reduce_scatter x1, waiting for transfers between devices, local(): lax.psum_scatter(partial_value, TP, scatter_dimension=2, tiled=True)  52.1 us
    reduce_scatter x2, waiting for transfers between devices, summed_rows(): nearer = lax.psum_scatter(x, axes[0], scatter_dimension=dim, tiled=True)  45.9 us
    all_to_all x1, blocking collectives, local(): lax.all_to_all(outgoing, 'ep', split_axis=0, concat_axis=0, tiled=True)  41.9 us
    psum x1, blocking collectives, local(): squares_out = lax.psum(jnp.sum(combined * combined, axis=1), TP)  26.3 us
    all_to_all x1, starting transfers between devices, local(): lax.all_to_all(back_send, 'ep', split_axis=0, concat_axis=0, tiled=True)  10.7 us
    all_to_all x1, starting transfers between devices, local(): lax.all_to_all(jnp.stack([tokens] * lax.axis_size(TP)), TP, 0, 0)  7.21 us
  transfers between devices with their start and end apart: 5, of which 4 were waited for; matrix products, arithmetic and copies ran while one was open for 3% of the time, Pallas kernels for 0%

profile of v1, /device:TPU:2, one launch (start us, length us, event | category | flops | bytes accessed | tf_op | source)
XLA Modules:
  0.0 222.7 jit_solution(2544578256830319529)
XLA Ops:
  6.5 1.4 stack.2
  7.9 7.2 %all-to-all-start = ((bf16[16,8,256]{2,1,0:T(8,128)(2,1)}), bf16[16,8,256]{2,1,0:T(8,128)(2,1)S(1)}, u32[]{:S(2)}, u32[]{:S(2)}) async-start(bf16[16,8,256]{2,1,0:T(8,128)(2,1)} %stack.2), calls=%async_computation | async-start | bytes 131072 | tf_op jit(solution)/shard_map/all_to_all | solution.py:37
  15.2 0.7 reduce_max.9
  15.9 0.7 fusion.23
  16.6 0.8 copy.34
  17.4 0.1 eq.30
  17.5 0.2 select_reduce_fusion.1
  17.8 0.7 fusion.22
  18.7 4.3 %all-to-all-done = bf16[16,8,256]{2,1,0:T(8,128)(2,1)S(1)} async-done(((bf16[16,8,256]{2,1,0:T(8,128)(2,1)}), bf16[16,8,256]{2,1,0:T(8,128)(2,1)S(1)}, u32[]{:S(2)}, u32[]{:S(2)}) %all-to-all-start) | async-done | bytes 65568 | tf_op jit(solution)/shard_map/all_to_all | solution.py:37
  22.9 0.1 multiply_reduce_fusion
  23.1 0.8 multiply_convert_fusion
  23.9 0.5 convolution_convert_fusion
  24.4 0.4 all_to_all.18
  24.8 41.9 %all_to_all.26 = bf16[32,4,4096]{2,1,0:T(4,128)(2,1)S(1)} all-to-all(bf16[32,4,4096]{2,1,0:T(4,128)(2,1)S(1)} %all_to_all.18), channel_id=1, replica_groups=mesh['ep'=32,'tp_0'=8,'tp_1'=2] {'ep'}, dimensions={0} | all-to-all | bytes 2097152 | tf_op jit(solution)/shard_map/all_to_all | solution.py:74
  66.7 0.5 reshape.73
  67.3 2.0 copy.41
  69.3 1.6 reshape.74
  70.9 0.4 fusion.26
  71.3 3.4 %fusion.1 = f32[2,64,4096]{2,1,0:T(8,128)} fusion(bf16[2,64,4096]{2,1,0:T(8,128)(2,1)S(1)} %copy-done, bf16[2,64,4096]{2,1,0:T(8,128)(2,1)S(1)} %reshape.74, bf16[2,4096,64]{1,2,0:T(8,128)(2,1)} %param.17, f32[2,64,64]{2,1,0:T(8,128)S(1)} %fusion.26), kind=kOutput, calls=%fused_computation.3 | convolution fusion | flops 134266880 | bytes 5275648 | tf_op jit(solution)/shard_map/erf,efd->erd/dot_general | solution.py:83
  74.8 0.9 copy-done.2
  75.7 0.2 fusion.27
  76.0 1.2 fusion.3
  77.3 52.1 %reduce-scatter.4.cloned.1.call-done = f32[2,64,256]{2,1,0:T(8,128)} async-done(((f32[2,64,4096]{2,1,0:T(8,128)}), f32[2,64,256]{2,1,0:T(8,128)}) %reduce-scatter.4.cloned.1.call-update) | async-done | bytes 131088 | tf_op jit(solution)/shard_map/reduce_scatter | solution.py:86
  129.4 1.0 reshape.75
  130.4 0.7 copy.39
  131.1 10.7 %all-to-all-start.2 = ((f32[32,4,256]{2,1,0:T(4,128)}), f32[32,4,256]{2,1,0:T(4,128)S(1)}, u32[]{:S(2)}, u32[]{:S(2)}) async-start(f32[32,4,256]{2,1,0:T(4,128)} %copy.39), calls=%async_computation.3 | async-start | bytes 262144 | tf_op jit(solution)/shard_map/all_to_all | solution.py:92
  141.9 28.9 %reduce-scatter.6.cloned.1.call-done = f32[8,512]{1,0:T(8,128)} async-done(((f32[8,4096]{1,0:T(8,128)}), f32[8,512]{1,0:T(8,128)}) %reduce-scatter.6.cloned.1.call-update) | async-done | bytes 16400 | tf_op jit(solution)/shard_map/reduce_scatter | solution.py:15
  170.8 0.2 fusion.7
  171.1 17.1 %reduce-scatter.8.cloned.1.call-done = f32[8,256]{1,0:T(8,128)} async-done(((f32[8,512]{1,0:T(8,128)}), f32[8,256]{1,0:T(8,128)}) %reduce-scatter.8.cloned.1.call-update) | async-done | bytes 8208 | tf_op jit(solution)/shard_map/reduce_scatter | solution.py:15
  188.2 1.0 multiply_reduce_fusion.1
  189.1 26.3 %psum.7 = f32[8]{0:T(128)S(1)} all-reduce(f32[8]{0:T(128)S(1)} %get-tuple-element.7), channel_id=1, replica_groups=mesh['ep'=32,'tp_0'=8,'tp_1'=2] {'tp_0','tp_1'}, use_global_device_ids=true, to_apply=%region_11.12 | all-reduce | flops 8 | bytes 64 | tf_op jit(solution)/shard_map/psum | solution.py:99
  215.5 0.7 multiply_convert_fusion.1
  (31 shorter events, 0.8 us)
Async XLA Ops:
  6.5 64.7 %copy-start = (bf16[2,64,4096]{2,1,0:T(8,128)(2,1)S(1)}, bf16[2,64,4096]{2,1,0:T(8,128)(2,1)}, u32[]{:S(2)}) copy-start(bf16[2,64,4096]{2,1,0:T(8,128)(2,1)} %param.18) | copy-start | bytes 3145732
  7.9 15.0 %all-to-all-start = ((bf16[16,8,256]{2,1,0:T(8,128)(2,1)}), bf16[16,8,256]{2,1,0:T(8,128)(2,1)S(1)}, u32[]{:S(2)}, u32[]{:S(2)}) async-start(bf16[16,8,256]{2,1,0:T(8,128)(2,1)} %stack.2), calls=%async_computation | async-start | bytes 131072 | tf_op jit(solution)/shard_map/all_to_all | solution.py:37
  15.1 114.2 %reduce-scatter.4.cloned.1.call-start = ((), (), s32[]{:S(2)}) async-start(), calls=%async_computation.6 | async-start | bytes 2228224 | tf_op jit(solution)/shard_map/reduce_scatter | solution.py:86
  69.3 1.6 copy-start.1
  74.7 1.0 copy-start.2
  74.7 1.3 copy-start.3
  74.7 1.4 copy-start.4
  74.7 96.1 %copy-start.6 = (f32[4096]{0:T(1024)S(1)}, f32[4096]{0:T(1024)}, u32[]{:S(2)}) copy-start(f32[4096]{0:T(1024)} %param.22) | copy-start | bytes 49156
  74.7 140.8 %copy-start.5 = (f32[256]{0:T(256)S(1)}, f32[256]{0:T(256)}, u32[]{:S(2)}) copy-start(f32[256]{0:T(256)} %param.23) | copy-start | bytes 3076
  74.7 96.0 %reduce-scatter.6.cloned.1.call-start = ((), (), s32[]{:S(2)}) async-start(), calls=%async_computation.7 | async-start | bytes 147456 | tf_op jit(solution)/shard_map/reduce_scatter | solution.py:15
  131.1 40.0 %all-to-all-start.2 = ((f32[32,4,256]{2,1,0:T(4,128)}), f32[32,4,256]{2,1,0:T(4,128)S(1)}, u32[]{:S(2)}, u32[]{:S(2)}) async-start(f32[32,4,256]{2,1,0:T(4,128)} %copy.39), calls=%async_computation.3 | async-start | bytes 262144 | tf_op jit(solution)/shard_map/all_to_all | solution.py:92
  141.8 46.4 %reduce-scatter.8.cloned.1.call-start = ((), (), s32[]{:S(2)}) async-start(), calls=%async_computation.8 | async-start | bytes 24576 | tf_op jit(solution)/shard_map/reduce_scatter | solution.py:15
Sparse Core Ops, SparseCore 0:
  74.8 54.4 reduce-scatter.3
  132.1 38.5 reduce-scatter.5
  173.5 14.6 reduce-scatter.7
